TPU v7x, 32 devices: a whole 2x2x4 slice. The times are simulated.
32 devices in a mesh: sp: 8 (over z, core), tp: 4 (over y, x).
Axes of the slice: x: 2, y: 2, z: 4, core: 2. Of those that a mesh axis runs over, the one named last changes fastest.
Arguments:
- stream: bfloat16 [1024, 2048], P('sp'), may hold values from -6 to 6
- query_small: bfloat16 [1024, 1024], P('sp', 'tp'), may hold values from -6 to 6
- key_small: bfloat16 [1024, 1024], P('sp', 'tp'), may hold values from -6 to 6
- value_small: bfloat16 [1024, 1024], P('sp', 'tp'), may hold values from -6 to 6
- query_large: bfloat16 [1024, 2048], P('sp', 'tp'), may hold values from -6 to 6
- key_large: bfloat16 [1024, 2048], P('sp', 'tp'), may hold values from -6 to 6
- value_large: bfloat16 [1024, 2048], P('sp', 'tp'), may hold values from -6 to 6
- key_bias: bfloat16 [1024, 2, 16], P('sp', None, 'tp'), may hold values from -16 to 1
- out_small: bfloat16 [1024, 2048], P('tp'), may hold values from -0.75 to 0.75
- out_large: bfloat16 [2048, 2048], P('tp'), may hold values from -0.75 to 0.75
- gain_one: float32 [2048], replicated, may hold values from 0.1 to 1.9
- shift_one: float32 [2048], replicated, may hold values from -1.5 to 1.5
- gain_two: float32 [2048], replicated, may hold values from 0.1 to 1.9
- shift_two: float32 [2048], replicated, may hold values from -1.5 to 1.5
- expert_pick: int32 [1024, 2], P('sp'), may hold values from 0 to 7, as said below
- route_weight: float32 [1024, 2], P('sp'), may hold values from 0.2 to 1
- w_gate: bfloat16 [8, 2048, 4096], P('sp', None, 'tp'), may hold values from -0.125 to 0.125
- w_up: bfloat16 [8, 2048, 4096], P('sp', None, 'tp'), may hold values from -0.125 to 0.125
- w_down: bfloat16 [8, 4096, 2048], P('sp', 'tp'), may hold values from -0.09375 to 0.09375
Outputs:
- result: bfloat16 [1024, 2048], P(('sp', 'tp'))
Inputs may be any that keep to these rules, and one draw needn't show every extreme that they name: In each aligned block of 128 positions (the positions of one index of sp), no expert is named more than 64 times, and in every block some expert is named exactly 64 times. The two experts of a position differ and lie in one group: equal values of expert_pick // 2.
All inputs are finite; a program needn't handle non-finite values.
Results may differ from a plain program's by a relative error of at most 0.017.
Values may be sent and summed in bfloat16 or wider, within the bound.
A program may use at most 64 MiB of HBM per device.

v0:
```python
import functools

import jax
import jax.numpy as jnp
from jax import lax
from jax.experimental import pallas as pl
from jax.experimental.pallas import tpu as pltpu
from jax.sharding import PartitionSpec as P

HEAD_SMALL = 64
HEAD_LARGE = 128


ALPHA_RES = 2.0**0.25
NORM_EPS = 1e-05


def layer_norm(inputs, gain_vec, shift_vec):
    average = jnp.mean(inputs, axis=-1, keepdims=True)
    centred = inputs - average
    variance = jnp.mean(centred * centred, axis=-1, keepdims=True)
    return centred * lax.rsqrt(variance + NORM_EPS) * gain_vec + shift_vec


def stick_group(queries, key_rows, value_rows, log_bias, position):
    query_count = queries.shape[0]
    head_count = queries.shape[1]
    value_size = value_rows.shape[2]
    key_span = 4 * query_count
    score_scale = queries.shape[2] ** (-0.5)
    query_pos = position * query_count + jnp.arange(query_count, dtype=jnp.int32)
    block_count = (position * query_count + query_count + key_span - 1) // key_span

    def visit_block(turn_index, carry):
        running, stay_sum = carry
        first_key = (block_count - 1 - turn_index) * key_span
        key_block = lax.dynamic_slice_in_dim(key_rows, first_key, key_span, 0)
        value_block = lax.dynamic_slice_in_dim(value_rows, first_key, key_span, 0)
        bias_block = lax.dynamic_slice_in_dim(log_bias, first_key, key_span, 0).astype(jnp.float32)
        scores = jnp.einsum("qhd,khd->hqk", queries, key_block, preferred_element_type=jnp.float32)
        scores = scores * score_scale + bias_block.T[:, None, :]
        key_pos = first_key + jnp.arange(key_span, dtype=jnp.int32)
        causal = (key_pos[None, :] < query_pos[:, None])[None]
        log_stay = jnp.where(causal, jax.nn.log_sigmoid(-scores), 0.0)
        later_sum = lax.cumsum(log_stay, axis=2, reverse=True) - log_stay + stay_sum[:, :, None]
        stick_weight = jnp.where(
            causal, jnp.exp(jax.nn.log_sigmoid(scores) + later_sum), 0.0
        ).astype(jnp.bfloat16)
        running = running + jnp.einsum(
            "hqk,khd->qhd", stick_weight, value_block, preferred_element_type=jnp.float32
        )
        stay_sum = stay_sum + jnp.sum(log_stay, axis=2)
        return (running, stay_sum)

    start_total = jnp.zeros((query_count, head_count, value_size), jnp.float32)
    start_stay = jnp.zeros((head_count, query_count), jnp.float32)
    running, stay_sum = lax.fori_loop(0, block_count, visit_block, (start_total, start_stay))
    return running.reshape(query_count, head_count * value_size).astype(jnp.bfloat16)


def split_heads(array, head_size):
    return array.reshape(array.shape[0], array.shape[1] // head_size, head_size)


def local(
    stream,
    query_small,
    key_small,
    value_small,
    query_large,
    key_large,
    value_large,
    key_bias,
    out_small,
    out_large,
    gain_one,
    shift_one,
    gain_two,
    shift_two,
    expert_pick,
    route_weight,
    w_gate,
    w_up,
    w_down,
):
    row_count = stream.shape[0]
    position = lax.axis_index("sp")
    gathered = (
        lax.all_gather(key_small, "sp", axis=0, tiled=True),
        lax.all_gather(value_small, "sp", axis=0, tiled=True),
        lax.all_gather(key_large, "sp", axis=0, tiled=True),
        lax.all_gather(value_large, "sp", axis=0, tiled=True),
        lax.all_gather(key_bias, "sp", axis=0, tiled=True),
    )
    att_small = stick_group(
        split_heads(query_small, HEAD_SMALL),
        split_heads(gathered[0], HEAD_SMALL),
        split_heads(gathered[1], HEAD_SMALL),
        gathered[4][:, 0],
        position,
    )
    att_large = stick_group(
        split_heads(query_large, HEAD_LARGE),
        split_heads(gathered[2], HEAD_LARGE),
        split_heads(gathered[3], HEAD_LARGE),
        gathered[4][:, 1],
        position,
    )
    partial_value = jnp.dot(att_small, out_small, preferred_element_type=jnp.float32)
    partial_value = partial_value + jnp.dot(
        att_large, out_large, preferred_element_type=jnp.float32
    )
    mixer_out = lax.psum(partial_value.astype(jnp.bfloat16), "tp").astype(jnp.float32)
    normed = layer_norm(
        ALPHA_RES * stream.astype(jnp.float32) + mixer_out, gain_one, shift_one
    ).astype(jnp.bfloat16)
    experts = w_gate.shape[0] * lax.axis_size("sp")
    capacity = 4 * row_count // experts
    tp_count = lax.axis_size("tp")
    tp_index = lax.axis_index("tp")
    per_lane = capacity // tp_count
    flat_picks = expert_pick.reshape(-1)
    one_hot = (flat_picks[:, None] == jnp.arange(experts, dtype=jnp.int32)[None, :]).astype(
        jnp.int32
    )
    slot_rank = jnp.sum((jnp.cumsum(one_hot, axis=0) - one_hot) * one_hot, axis=1)
    slot_index = (flat_picks * capacity + slot_rank).reshape(row_count, 2)

    def selector(first_slot, slot_count):
        target = (
            jnp.arange(experts, dtype=jnp.int32)[:, None] * capacity
            + first_slot
            + jnp.arange(slot_count, dtype=jnp.int32)[None, :]
        ).reshape(-1)
        return [target[:, None] == slot_index[None, :, pick_index] for pick_index in range(2)]

    own_select = selector(tp_index * per_lane, per_lane)
    all_select = selector(0, capacity)
    placing = (all_select[0] | all_select[1]).astype(jnp.bfloat16)
    outgoing = jnp.dot(placing, normed, preferred_element_type=jnp.float32).astype(jnp.bfloat16)
    arrived = lax.all_to_all(
        outgoing.reshape(experts, capacity, normed.shape[1]),
        "sp",
        split_axis=0,
        concat_axis=0,
        tiled=True,
    )
    flat_rows = arrived.reshape(-1, arrived.shape[2])
    gate = jnp.dot(flat_rows, w_gate[0], preferred_element_type=jnp.float32)
    upper = jnp.dot(flat_rows, w_up[0], preferred_element_type=jnp.float32)
    hidden = (jax.nn.silu(gate) * upper).astype(jnp.bfloat16)
    expert_terms = jnp.dot(hidden, w_down[0], preferred_element_type=jnp.float32).reshape(
        arrived.shape
    )
    summed = lax.psum_scatter(
        expert_terms.astype(jnp.bfloat16), "tp", scatter_dimension=1, tiled=True
    )
    returned = lax.all_to_all(summed, "sp", split_axis=0, concat_axis=0, tiled=True).reshape(
        experts * per_lane, normed.shape[1]
    )
    picked_first = jnp.einsum(
        "sr,sd->rd",
        own_select[0].astype(jnp.bfloat16),
        returned,
        preferred_element_type=jnp.float32,
    )
    picked_second = jnp.einsum(
        "sr,sd->rd",
        own_select[1].astype(jnp.bfloat16),
        returned,
        preferred_element_type=jnp.float32,
    )
    partial_mix = route_weight[:, 0:1] * picked_first + route_weight[:, 1:2] * picked_second
    expert_mix = lax.psum_scatter(
        partial_mix.astype(jnp.bfloat16), "tp", scatter_dimension=0, tiled=True
    ).astype(jnp.float32)
    own_count = row_count // tp_count
    own_rows = lax.dynamic_slice_in_dim(normed, tp_index * own_count, own_count, 0).astype(
        jnp.float32
    )
    return layer_norm(ALPHA_RES * own_rows + expert_mix, gain_two, shift_two).astype(jnp.bfloat16)


GROUPS = 4


def fast_kernel(
    dims,
    qs_ref, ks_ref, vs_ref, ql_ref, kl_ref, vl_ref, bias_ref, stream_ref, os_ref, ol_ref,
    g1_ref, b1_ref, g2_ref, b2_ref, pick_ref, route_ref, wg_ref, wu_ref, wd_ref,
    out_ref,
    pack_a, pack_v, rq, rk, rv, rb, aq, ak, ao, ra, wos, wol, strm, pb, rp, st, rst, normed,
    place, xs, wsend, wrecv, ag, wg, wu, wd, hid, own_y, cs, cr, ts, rr, zs, zr, fs, fr,
    load_sem, q_send, q_recv, a_send, a_recv, p_send, p_recv, s_send, s_recv,
    x_send, x_recv, w_send, w_recv, g_send, g_recv, h_send, h_recv, c_send, c_recv,
    t_send, t_recv, z_send, z_recv, f_send, f_recv,
):
    n_sp, n_tp, rows, cols, cap, small_heads, hs, hl = dims
    f32, bf16 = jnp.float32, jnp.bfloat16
    sp = lax.axis_index("sp")
    tp = lax.axis_index("tp")
    core = lax.rem(sp, 2)
    chip = lax.div(sp, 2)
    sibling = sp + 1 - 2 * core
    n_z = n_sp // 2
    is_small = sp < small_heads
    large_heads = n_sp - small_heads
    ffw = wg_ref.shape[2]
    width = n_tp * cols

    def mesh_copy(src, dst, send, recv, target):
        return pltpu.make_async_remote_copy(
            src_ref=src, dst_ref=dst, send_sem=send, recv_sem=recv,
            device_id=target, device_id_type=pl.DeviceIdType.MESH,
        )

    def sp_at(j):
        return (j, tp)

    def tp_at(j):
        return (sp, j)

    def flip(index, mask, count):
        total, bit = 0, 1
        while bit < count:
            digit = lax.rem(lax.div(index, bit), 2)
            total = total + bit * (1 - digit if mask & bit else digit)
            bit *= 2
        return total

    z_masks = [0, n_z - 1, *range(1, n_z - 1)]
    z_order = [flip(chip, m, n_z) for m in z_masks]
    peers = [flip(tp, m, n_tp) for m in range(n_tp)]
    out_peers = [*peers[:0:-1], peers[0]]

    barrier = pltpu.get_barrier_semaphore()
    for k in range(1, n_sp):
        pl.semaphore_signal(barrier, inc=1, device_id=sp_at(lax.rem(sp + k, n_sp)), device_id_type=pl.DeviceIdType.MESH)
    for k in range(1, n_tp):
        pl.semaphore_signal(barrier, inc=1, device_id=tp_at(lax.rem(tp + k, n_tp)), device_id_type=pl.DeviceIdType.MESH)

    own_cols = pl.ds(pl.multiple_of(tp * cols, cols), cols)
    loads = [
        pltpu.make_async_copy(os_ref, wos, load_sem.at[0]),
        pltpu.make_async_copy(ol_ref, wol, load_sem.at[1]),
        pltpu.make_async_copy(stream_ref.at[:, own_cols], strm, load_sem.at[2]),
        pltpu.make_async_copy(wg_ref.at[0], wg, load_sem.at[3]),
        pltpu.make_async_copy(wu_ref.at[0], wu, load_sem.at[4]),
        pltpu.make_async_copy(wd_ref.at[0], wd, load_sem.at[5]),
    ]
    for load in loads:
        load.start()

    for h in range(small_heads):
        part = slice(h * hs, (h + 1) * hs)
        pack_a[h] = jnp.concatenate([qs_ref[:, part], ks_ref[:, part]], axis=1)
        pack_v[h] = jnp.concatenate([vs_ref[:rows // 2, part], vs_ref[rows // 2:, part]], axis=1)

    pl.semaphore_wait(barrier, n_sp + n_tp - 2)

    half_block = pl.ds(0, rows // 2)

    def head_copies(j, slot):
        if j < small_heads:
            pairs = [(0, pack_a.at[j], rq.at[slot]), (2, pack_v.at[j], rv.at[slot, half_block])]
        else:
            part = pl.ds((j - small_heads) * hl, hl)
            pairs = [
                (0, ql_ref.at[:, part], rq.at[slot]),
                (1, kl_ref.at[:, part], rk.at[slot]),
                (2, vl_ref.at[:, part], rv.at[slot]),
            ]
        pairs.append((3, bias_ref.at[j], rb.at[slot]))
        return pairs

    for distance in range(n_z):
        for j in range(n_sp):
            hops = jnp.maximum(j // 2 - chip, chip - j // 2)

            @pl.when((hops == distance) & (j != sp))
            def _():
                for kind, src, dst in head_copies(j, sp):
                    mesh_copy(src, dst, q_send.at[kind, j], q_recv.at[kind, sp], sp_at(j)).start()

    for j in range(n_sp):
        @pl.when(j == sp)
        def _():
            for kind, src, dst in head_copies(j, j):
                pltpu.make_async_copy(src, dst, q_recv.at[kind, j]).start()

    group = lax.div(pick_ref[0:1, :], 2)
    first_even = lax.rem(pick_ref[0:1, :], 2) == 0
    sub8 = lax.broadcasted_iota(jnp.int32, (8, rows), 0)
    one_hot = (sub8 == group).astype(f32)
    sub_r = lax.broadcasted_iota(jnp.int32, (rows, rows), 0)
    lane_r = lax.broadcasted_iota(jnp.int32, (rows, rows), 1)
    before = (sub_r < lane_r).astype(f32).astype(bf16)
    counts = jnp.dot(one_hot.astype(bf16), before, preferred_element_type=f32)
    rank = jnp.sum(one_hot * counts, axis=0, keepdims=True).astype(jnp.int32)
    slot_row = group * cap + rank
    slot_iota = lax.broadcasted_iota(jnp.int32, (GROUPS * cap, rows), 0)
    place[...] = (slot_iota == slot_row).astype(f32).astype(bf16)
    w_even = jnp.where(first_even, route_ref[0:1, :], route_ref[1:2, :])
    w_odd = jnp.where(first_even, route_ref[1:2, :], route_ref[0:1, :])
    w8 = jnp.where(sub8 == 0, w_even, jnp.where(sub8 == 1, w_odd, 0.0))
    w_hi = w8.astype(bf16)
    w_lo = (w8 - w_hi.astype(f32)).astype(bf16)
    for g in range(GROUPS):
        pick_g = ((sub_r == slot_row - g * cap) & (sub_r < cap)).astype(f32).astype(bf16)
        last = (((1,), (1,)), ((), ()))
        wsend[g] = lax.dot_general(w_hi, pick_g, last, preferred_element_type=f32) + lax.dot_general(
            w_lo, pick_g, last, preferred_element_type=f32
        )

    for j in range(n_sp):
        for kind in (0, 3):
            dst = (rq, None, None, rb)[kind].at[j]
            pltpu.make_async_copy(dst, dst, q_recv.at[kind, j]).wait()

    def unfold(packed):
        tall = jnp.concatenate([packed[:, :hs], packed[:, hs:]], axis=0)
        return jnp.concatenate([tall, jnp.zeros_like(tall)], axis=1)

    @pl.when(jnp.logical_not(is_small))
    def _():
        for j in range(n_sp):
            pltpu.make_async_copy(rk.at[j], rk.at[j], q_recv.at[1, j]).wait()
            pltpu.make_async_copy(rv.at[j], rv.at[j], q_recv.at[2, j]).wait()
            aq[pl.ds(j * rows, rows), :] = rq[j]
            ak[pl.ds(j * rows, rows), :] = rk[j]

    @pl.when(is_small)
    def _():
        lane = lax.broadcasted_iota(jnp.int32, (rows, hl), 1)
        for j in range(n_sp):
            folded = rv.at[j, half_block]
            pltpu.make_async_copy(folded, folded, q_recv.at[2, j]).wait()
            rv[j] = unfold(folded[...])
            both = rq[j]
            aq[pl.ds(j * rows, rows), :] = jnp.where(lane < hs, both, jnp.zeros_like(both))
            ak[pl.ds(j * rows, rows), :] = jnp.concatenate([both[:, hs:], both[:, :hs]], axis=1)

    for j in range(n_sp):
        @pl.when(j != sp)
        def _():
            for kind, src, dst in head_copies(j, sp):
                mesh_copy(src, dst, q_send.at[kind, j], q_recv.at[kind, sp], sp_at(j)).wait_send()

    scale = jnp.where(is_small, hs**-0.5, hl**-0.5).astype(f32)
    span = 2 * rows
    sub_t = lax.broadcasted_iota(jnp.int32, (span, span), 0)
    lane_t = lax.broadcasted_iota(jnp.int32, (span, span), 1)
    tri = (sub_t >= lane_t).astype(f32).astype(bf16)
    causal = lane_t < sub_t

    def tile(query, kj, diagonal, total, later):
        keys = ak[pl.ds(pl.multiple_of(kj * span, span), span), :]
        log_odds = jnp.concatenate([rb[2 * kj, 0:1, :], rb[2 * kj + 1, 0:1, :]], axis=1)
        score = lax.dot_general(query, keys, (((1,), (1,)), ((), ())), preferred_element_type=f32)
        score = score * scale + log_odds
        soft = jnp.maximum(score, 0.0) + jnp.log(1.0 + jnp.exp(-jnp.abs(score)))
        if diagonal:
            soft = jnp.where(causal, soft, 0.0)
        high = soft.astype(bf16)
        low = (soft - high.astype(f32)).astype(bf16)
        run = jnp.dot(high, tri, preferred_element_type=f32) + jnp.dot(low, tri, preferred_element_type=f32)
        stick = jnp.exp(score - run - later)
        if diagonal:
            stick = jnp.where(causal, stick, 0.0)
        values = jnp.concatenate([rv[2 * kj], rv[2 * kj + 1]], axis=0)
        total = total + jnp.dot(stick.astype(bf16), values, preferred_element_type=f32)
        return total, later + run[:, 0:1]

    def head_back(d, small):
        src, dst = (ao.at[d, half_block], ra.at[sp, half_block]) if small else (ao.at[d], ra.at[sp])
        return mesh_copy(src, dst, a_send.at[d], a_recv.at[sp], sp_at(d))

    for qi in range(n_sp // 2):
        query = aq[qi * span:(qi + 1) * span, :]
        carry = tile(query, qi, True, jnp.zeros((span, hl), f32), jnp.zeros((span, 1), f32))
        if qi:
            def visit(turn, carry):
                return tile(query, qi - 1 - turn, False, *carry)
            carry = lax.fori_loop(0, qi, visit, carry)
        for half in range(2):
            d = 2 * qi + half
            block = carry[0][half * rows:(half + 1) * rows].astype(bf16)

            @pl.when(is_small)
            def _():
                ao[d, :rows // 2, :] = jnp.concatenate([block[:rows // 2, :hs], block[rows // 2:, :hs]], axis=1)

            @pl.when(jnp.logical_not(is_small))
            def _():
                ao[d] = block
        for half in range(2):
            d = 2 * qi + half
            for small in (True, False):
                @pl.when((d != sp) & (is_small if small else jnp.logical_not(is_small)))
                def _():
                    head_back(d, small).start()

            if d < small_heads:
                own = pltpu.make_async_copy(ao.at[d, half_block], ra.at[d, half_block], a_recv.at[d])
            else:
                own = pltpu.make_async_copy(ao.at[d], ra.at[d], a_recv.at[d])

            @pl.when(d == sp)
            def _():
                own.start()

    for load in loads[:3]:
        load.wait()
    for j in range(n_sp):
        landed = ra.at[j, half_block] if j < small_heads else ra.at[j]
        pltpu.make_async_copy(landed, landed, a_recv.at[j]).wait()
    att_small = jnp.concatenate([unfold(ra[j, :rows // 2, :])[:, :hs] for j in range(small_heads)], axis=1)
    att_large = jnp.concatenate([ra[j] for j in range(small_heads, n_sp)], axis=1)

    def tp_wait_recv(buf, sem, src):
        pltpu.make_async_copy(buf.at[src], buf.at[src], sem.at[src]).wait()

    for k in range(1, n_tp + 1):
        t = out_peers[k - 1]
        part = pl.ds(pl.multiple_of(t * cols, cols), cols)
        term = jnp.dot(att_small, wos[:, part], preferred_element_type=f32)
        term = term + jnp.dot(att_large, wol[:, part], preferred_element_type=f32)
        pb[k - 1] = term.astype(bf16)
        if k < n_tp:
            mesh_copy(pb.at[k - 1], rp.at[tp], p_send.at[k], p_recv.at[tp], tp_at(t)).start()
    mixed = ALPHA_RES * strm[...].astype(f32) + pb[n_tp - 1].astype(f32)
    for k in range(1, n_tp):
        src = lax.rem(tp + k, n_tp)
        tp_wait_recv(rp, p_recv, src)
        mixed = mixed + rp[src].astype(f32)

    eye = sub_r == lane_r

    def to_row(column):
        return jnp.sum(jnp.where(eye, column, 0.0), axis=0, keepdims=True)

    def to_column(row):
        return jnp.sum(jnp.where(eye, row, 0.0), axis=1, keepdims=True)

    own_mean = jnp.mean(mixed, axis=1, keepdims=True)
    centred = mixed - own_mean
    own_square = jnp.sum(centred * centred, axis=1, keepdims=True)
    mean_row, square_row = to_row(own_mean), to_row(own_square)
    st[...] = jnp.where(sub8 == 0, mean_row, square_row)
    for k in range(1, n_tp):
        t = lax.rem(tp + k, n_tp)
        mesh_copy(st, rst.at[tp], s_send.at[k], s_recv.at[tp], tp_at(t)).start()
    means, squares = [mean_row], [square_row]
    for k in range(1, n_tp):
        src = lax.rem(tp + k, n_tp)
        tp_wait_recv(rst, s_recv, src)
        means.append(rst[src, 0:1, :])
        squares.append(rst[src, 1:2, :])
    full_mean = sum(means) / n_tp
    spread = sum(squares) + cols * sum((m - full_mean) * (m - full_mean) for m in means)
    scale_row = lax.rsqrt(spread / width + NORM_EPS)
    norm_val = (mixed - to_column(full_mean)) * to_column(scale_row) * g1_ref[:, own_cols] + b1_ref[:, own_cols]
    normed[...] = norm_val.astype(bf16)

    for g in range(GROUPS):
        xs[g] = jnp.dot(place[g * cap:(g + 1) * cap, :], normed[...], preferred_element_type=f32).astype(bf16)
    for k in range(n_z):
        g = z_order[k]
        dst = ag.at[core, tp, chip]
        if k == 0:
            pltpu.make_async_copy(xs.at[g], dst, x_recv.at[chip]).start()
        else:
            mesh_copy(xs.at[g], dst, x_send.at[k], x_recv.at[chip], sp_at(2 * g + core)).start()
    for k in range(n_sp):
        j = lax.rem(sp + k, n_sp)
        if k == 0:
            pltpu.make_async_copy(wsend.at[chip], wrecv.at[sp], w_recv.at[sp]).start()
        else:
            mesh_copy(wsend.at[lax.div(j, 2)], wrecv.at[sp], w_send.at[k], w_recv.at[sp], sp_at(j)).start()

    for z in z_order:
        piece = ag.at[core, tp, z]
        pltpu.make_async_copy(piece, piece, x_recv.at[z]).wait()
        for m in range(1, n_tp):
            mesh_copy(piece, piece, g_send.at[m, z], g_recv.at[tp, z], tp_at(peers[m])).start()
        mesh_copy(piece, piece, h_send.at[tp, z], h_recv.at[tp, z], sp_at(sibling)).start()
    for j in range(n_sp):
        pltpu.make_async_copy(wrecv.at[j], wrecv.at[j], w_recv.at[j]).wait()
    for load in loads[3:]:
        load.wait()

    other = 1 - core
    lane_c = lax.broadcasted_iota(jnp.int32, (cap, rows), 1)
    sub_c = lax.broadcasted_iota(jnp.int32, (cap, rows), 0)
    step = min(256, ffw)
    half = (n_z // 2) * cap

    def slot_weights(c, z):
        row = wrecv[2 * z + c, pl.ds(core, 1), :]
        return jnp.sum(jnp.where(sub_c == lane_c, row, 0.0), axis=1, keepdims=True)

    for p in range(2):
        zs_p = z_order[p * (n_z // 2):(p + 1) * (n_z // 2)]
        for z in zs_p:
            for m in range(1, n_tp):
                piece = ag.at[core, peers[m], z]
                pltpu.make_async_copy(piece, piece, g_recv.at[peers[m], z]).wait()
                mesh_copy(piece, piece, h_send.at[peers[m], z], h_recv.at[peers[m], z], sp_at(sibling)).start()
        for z in zs_p:
            for t in range(n_tp):
                piece = ag.at[other, t, z]
                pltpu.make_async_copy(piece, piece, h_recv.at[t, z]).wait()
        weights = jnp.concatenate([slot_weights(c, z) for c in (other, core) for z in zs_p], axis=0)

        def body(n, carry):
            part = pl.ds(pl.multiple_of(n * step, step), step)
            gate = jnp.zeros((2 * half, step), f32)
            upper = jnp.zeros((2 * half, step), f32)
            for t in range(n_tp):
                x = jnp.concatenate([ag[c, t, z] for c in (other, core) for z in zs_p], axis=0)
                gate = gate + jnp.dot(x, wg[t * cols:(t + 1) * cols, part], preferred_element_type=f32)
                upper = upper + jnp.dot(x, wu[t * cols:(t + 1) * cols, part], preferred_element_type=f32)
            hid[:, part] = (gate / (1.0 + jnp.exp(-gate)) * upper).astype(bf16)
            return carry

        lax.fori_loop(0, ffw // step, body, 0)

        def join(k):
            pltpu.make_async_copy(cr.at[p, k], cr.at[p, k], c_recv.at[p, k]).wait()
            both = own_y[p, k] + cr[p, k].astype(f32)
            if k == n_tp - 1:
                own_y[p, k] = both
                return
            for i in range(n_z // 2):
                kz = p * (n_z // 2) + i
                ts[k, kz] = both[i * cap:(i + 1) * cap].astype(bf16)
                mesh_copy(
                    ts.at[k, kz], rr.at[tp, kz], t_send.at[k, kz], t_recv.at[tp, kz], tp_at(out_peers[k])
                ).start()

        for k in range(n_tp):
            part = pl.ds(pl.multiple_of(out_peers[k] * cols, cols), cols)
            y = jnp.dot(hid[...], wd[:, part], preferred_element_type=f32) * weights
            cs[p, k] = y[:half].astype(bf16)
            mesh_copy(cs.at[p, k], cr.at[p, k], c_send.at[p, k], c_recv.at[p, k], sp_at(sibling)).start()
            own_y[p, k] = y[half:]
            if k:
                join(k - 1)
        join(n_tp - 1)

    for kz in range(n_z):
        z = z_order[kz]
        i = kz % (n_z // 2)
        total = own_y[kz // (n_z // 2), n_tp - 1, i * cap:(i + 1) * cap, :]
        for m in range(1, n_tp):
            src = peers[m]
            pltpu.make_async_copy(rr.at[src, kz], rr.at[src, kz], t_recv.at[src, kz]).wait()
            total = total + rr[src, kz].astype(f32)
        zs[kz] = total.astype(bf16)
        if kz:
            mesh_copy(zs.at[kz], zr.at[chip], z_send.at[kz], z_recv.at[chip], sp_at(2 * z + core)).start()
        else:
            pltpu.make_async_copy(zs.at[kz], zr.at[chip], z_recv.at[chip]).start()
    for z in range(n_z):
        pltpu.make_async_copy(zr.at[z], zr.at[z], z_recv.at[z]).wait()
    expert_mix = lax.dot_general(
        place[...], zr[...].reshape(n_z * cap, cols), (((0,), (0,)), ((), ())), preferred_element_type=f32
    )
    final = ALPHA_RES * normed[...].astype(f32) + expert_mix
    own_rows = rows // n_tp
    for t in range(n_tp):
        fs[t] = final[t * own_rows:(t + 1) * own_rows]
    for k in range(1, n_tp):
        t = lax.rem(tp + k, n_tp)
        mesh_copy(fs.at[t], fr.at[tp], f_send.at[k], f_recv.at[tp], tp_at(t)).start()
    keep = pltpu.make_async_copy(fs.at[tp], fr.at[tp], f_recv.at[tp])
    keep.start()
    for t in range(n_tp):
        tp_wait_recv(fr, f_recv, t)
    blocks = [fr[t] for t in range(n_tp)]
    average = sum(jnp.sum(b, axis=1, keepdims=True) for b in blocks) / width
    blocks = [b - average for b in blocks]
    variance = sum(jnp.sum(b * b, axis=1, keepdims=True) for b in blocks) / width
    inverse = lax.rsqrt(variance + NORM_EPS)
    for t in range(n_tp):
        part = slice(t * cols, (t + 1) * cols)
        out_ref[:, part] = (blocks[t] * inverse * g2_ref[:, part] + b2_ref[:, part]).astype(bf16)

    for d in range(n_sp):
        for small in (True, False):
            @pl.when((d != sp) & (is_small if small else jnp.logical_not(is_small)))
            def _():
                head_back(d, small).wait_send()
    for k in range(1, n_sp):
        j = lax.rem(sp + k, n_sp)
        mesh_copy(wsend.at[lax.div(j, 2)], wrecv.at[sp], w_send.at[k], w_recv.at[sp], sp_at(j)).wait_send()
    for k in range(1, n_tp):
        t = lax.rem(tp + k, n_tp)
        mesh_copy(pb.at[k - 1], rp.at[tp], p_send.at[k], p_recv.at[tp], tp_at(out_peers[k - 1])).wait_send()
        mesh_copy(st, rst.at[tp], s_send.at[k], s_recv.at[tp], tp_at(t)).wait_send()
        mesh_copy(fs.at[t], fr.at[tp], f_send.at[k], f_recv.at[tp], tp_at(t)).wait_send()
        for z in range(n_z):
            piece = ag.at[core, tp, z]
            mesh_copy(piece, piece, g_send.at[k, z], g_recv.at[tp, z], tp_at(peers[k])).wait_send()
            mesh_copy(
                ts.at[k - 1, z], rr.at[tp, z], t_send.at[k - 1, z], t_recv.at[tp, z], tp_at(out_peers[k - 1])
            ).wait_send()
    for k in range(1, n_z):
        g = z_order[k]
        mesh_copy(xs.at[g], ag.at[core, tp, chip], x_send.at[k], x_recv.at[chip], sp_at(2 * g + core)).wait_send()
        mesh_copy(zs.at[k], zr.at[chip], z_send.at[k], z_recv.at[chip], sp_at(2 * g + core)).wait_send()
    for t in range(n_tp):
        for p in range(2):
            mesh_copy(cs.at[p, t], cr.at[p, t], c_send.at[p, t], c_recv.at[p, t], sp_at(sibling)).wait_send()
        for z in range(n_z):
            piece = ag.at[core, t, z]
            mesh_copy(piece, piece, h_send.at[t, z], h_recv.at[t, z], sp_at(sibling)).wait_send()


def fast_local(
    stream, query_small, key_small, value_small, query_large, key_large, value_large, key_bias,
    out_small, out_large, gain_one, shift_one, gain_two, shift_two, expert_pick, route_weight,
    w_gate, w_up, w_down,
):
    f32, bf16 = jnp.float32, jnp.bfloat16
    n_sp, n_tp = lax.axis_size("sp"), lax.axis_size("tp")
    rows, width = stream.shape
    cols = width // n_tp
    hs, hl = HEAD_SMALL, HEAD_LARGE
    small_heads = query_small.shape[1] // hs
    cap = 4 * rows // (w_gate.shape[0] * n_sp)
    n_z = n_sp // 2
    ffw = w_gate.shape[2]
    bias = key_bias.astype(f32).transpose(1, 2, 0).reshape(n_sp, 1, rows)
    bias = jnp.broadcast_to(bias, (n_sp, 8, rows))
    vmem = pl.BlockSpec(memory_space=pltpu.VMEM)
    hbm = pl.BlockSpec(memory_space=pl.ANY)
    dma = pltpu.SemaphoreType.DMA
    V = pltpu.VMEM
    half = n_z * cap
    scratch = [
        V((small_heads, rows, hl), bf16), V((small_heads, rows // 2, hl), bf16),
        V((n_sp, rows, hl), bf16), V((n_sp, rows, hl), bf16), V((n_sp, rows, hl), bf16),
        V((n_sp, 8, rows), f32),
        V((n_sp * rows, hl), bf16), V((n_sp * rows, hl), bf16),
        V((n_sp, rows, hl), bf16), V((n_sp, rows, hl), bf16),
        V(out_small.shape, bf16), V(out_large.shape, bf16), V((rows, cols), bf16),
        V((n_tp, rows, cols), bf16), V((n_tp, rows, cols), bf16),
        V((8, rows), f32), V((n_tp, 8, rows), f32), V((rows, cols), bf16),
        V((GROUPS * cap, rows), bf16), V((GROUPS, cap, cols), bf16),
        V((GROUPS, 8, rows), f32), V((n_sp, 8, rows), f32),
        V((2, n_tp, n_z, cap, cols), bf16),
        V((width, ffw), bf16), V((width, ffw), bf16), V((ffw, width), bf16),
        V((half, ffw), bf16), V((2, n_tp, half // 2, cols), f32),
        V((2, n_tp, half // 2, cols), bf16), V((2, n_tp, half // 2, cols), bf16),
        V((n_tp - 1, n_z, cap, cols), bf16), V((n_tp, n_z, cap, cols), bf16),
        V((n_z, cap, cols), bf16), V((n_z, cap, cols), bf16),
        V((n_tp, rows // n_tp, cols), f32), V((n_tp, rows // n_tp, cols), f32),
        dma((6,)), dma((4, n_sp)), dma((4, n_sp)), dma((n_sp,)), dma((n_sp,)),
        dma((n_tp,)), dma((n_tp,)), dma((n_tp,)), dma((n_tp,)),
        dma((n_z,)), dma((n_z,)), dma((n_sp,)), dma((n_sp,)),
        dma((n_tp, n_z)), dma((n_tp, n_z)), dma((n_tp, n_z)), dma((n_tp, n_z)),
        dma((2, n_tp)), dma((2, n_tp)), dma((n_tp, n_z)), dma((n_tp, n_z)),
        dma((n_z,)), dma((n_z,)), dma((n_tp,)), dma((n_tp,)),
    ]
    dims = (n_sp, n_tp, rows, cols, cap, small_heads, hs, hl)
    return pl.pallas_call(
        functools.partial(fast_kernel, dims),
        out_shape=jax.ShapeDtypeStruct((rows // n_tp, width), bf16),
        in_specs=[vmem] * 7 + [hbm] * 3 + [vmem] * 6 + [hbm] * 3,
        out_specs=vmem,
        scratch_shapes=scratch,
        compiler_params=pltpu.CompilerParams(
            collective_id=0, has_side_effects=True, vmem_limit_bytes=60 * 1024 * 1024
        ),
        name="layer",
    )(
        query_small, key_small, value_small, query_large, key_large, value_large, bias,
        stream, out_small, out_large,
        gain_one[None], shift_one[None], gain_two[None], shift_two[None],
        expert_pick.T, route_weight.T, w_gate, w_up, w_down,
    )


def layer(*arrays):
    n_sp, n_tp = lax.axis_size("sp"), lax.axis_size("tp")
    heads = arrays[1].shape[1] // HEAD_SMALL + arrays[4].shape[1] // HEAD_LARGE
    experts = arrays[16].shape[0] * n_sp
    paired = experts == 2 * GROUPS and n_sp == experts
    if paired and heads == n_sp and arrays[7].shape[2] * 2 == n_sp and arrays[0].shape[1] % (128 * n_tp) == 0:
        return fast_local(*arrays)
    return local(*arrays)


def solution(mesh):
    placed = (
        P("sp", None),
        P("sp", "tp"),
        P("sp", "tp"),
        P("sp", "tp"),
        P("sp", "tp"),
        P("sp", "tp"),
        P("sp", "tp"),
        P("sp", None, "tp"),
        P("tp", None),
        P("tp", None),
        P(),
        P(),
        P(),
        P(),
        P("sp", None),
        P("sp", None),
        P("sp", None, "tp"),
        P("sp", None, "tp"),
        P("sp", "tp", None),
    )
    return jax.shard_map(
        layer, mesh=mesh, in_specs=placed, out_specs=P(("sp", "tp"), None), check_vma=False
    )
```

profile of v0, /device:TPU:0, one launch (start us, length us, event | category | flops | bytes accessed | tf_op | source)
XLA Modules:
  0.0 92.7 jit_solution(8507706162599944273)
XLA Ops:
  0.0 0.7 broadcast_in_dim.30
  0.7 0.6 broadcast_in_dim.24.bias_ref
  1.3 89.8 %layer.1 = bf16[32,2048]{1,0:T(8,128)(2,1)} custom-call(bf16[128,256]{1,0:T(8,128)(2,1)} %qs_ref.1, bf16[128,256]{1,0:T(8,128)(2,1)} %ks_ref.1, bf16[128,256]{1,0:T(8,128)(2,1)} %vs_ref.1, bf16[128,512]{1,0:T(8,128)(2,1)} %ql_ref.1, bf16[128,512]{1,0:T(8,128)(2,1)} %kl_ref.1, bf16[128,512]{1,0:T(8,128)(2,1)} %vl_ref.1, ...), custom_call_target="tpu_custom_call" | custom-call | tf_op jit(solution)/shard_map/layer/pallas_call | solution.py:667
  91.2 1.6 %copy.21 = bf16[32,2048]{1,0:T(8,128)(2,1)} copy(bf16[32,2048]{1,0:T(8,128)(2,1)} %layer.1) | data formatting | bytes 262144
where the time goes:
time: 92.9 us; the launch traced here: 92.7 us
  Pallas kernels  89.8 us (97%)
  local copies, waits for them, and re-layouts  2.19 us (2%)
    pallas_call x1, Pallas kernels, fast_local(): pl.pallas_call(functools.partial(fast_kernel, dims), out_shape=jax.ShapeD...  89.8 us

commit v1 on v0

v1 whole, which is shorter than its diff:
```python
import functools

import jax
import jax.numpy as jnp
from jax import lax
from jax.experimental import pallas as pl
from jax.experimental.pallas import tpu as pltpu
from jax.sharding import PartitionSpec as P

HEAD_SMALL = 64
HEAD_LARGE = 128


ALPHA_RES = 2.0**0.25
NORM_EPS = 1e-05


def layer_norm(inputs, gain_vec, shift_vec):
    average = jnp.mean(inputs, axis=-1, keepdims=True)
    centred = inputs - average
    variance = jnp.mean(centred * centred, axis=-1, keepdims=True)
    return centred * lax.rsqrt(variance + NORM_EPS) * gain_vec + shift_vec


def stick_group(queries, key_rows, value_rows, log_bias, position):
    query_count = queries.shape[0]
    head_count = queries.shape[1]
    value_size = value_rows.shape[2]
    key_span = 4 * query_count
    score_scale = queries.shape[2] ** (-0.5)
    query_pos = position * query_count + jnp.arange(query_count, dtype=jnp.int32)
    block_count = (position * query_count + query_count + key_span - 1) // key_span

    def visit_block(turn_index, carry):
        running, stay_sum = carry
        first_key = (block_count - 1 - turn_index) * key_span
        key_block = lax.dynamic_slice_in_dim(key_rows, first_key, key_span, 0)
        value_block = lax.dynamic_slice_in_dim(value_rows, first_key, key_span, 0)
        bias_block = lax.dynamic_slice_in_dim(log_bias, first_key, key_span, 0).astype(jnp.float32)
        scores = jnp.einsum("qhd,khd->hqk", queries, key_block, preferred_element_type=jnp.float32)
        scores = scores * score_scale + bias_block.T[:, None, :]
        key_pos = first_key + jnp.arange(key_span, dtype=jnp.int32)
        causal = (key_pos[None, :] < query_pos[:, None])[None]
        log_stay = jnp.where(causal, jax.nn.log_sigmoid(-scores), 0.0)
        later_sum = lax.cumsum(log_stay, axis=2, reverse=True) - log_stay + stay_sum[:, :, None]
        stick_weight = jnp.where(
            causal, jnp.exp(jax.nn.log_sigmoid(scores) + later_sum), 0.0
        ).astype(jnp.bfloat16)
        running = running + jnp.einsum(
            "hqk,khd->qhd", stick_weight, value_block, preferred_element_type=jnp.float32
        )
        stay_sum = stay_sum + jnp.sum(log_stay, axis=2)
        return (running, stay_sum)

    start_total = jnp.zeros((query_count, head_count, value_size), jnp.float32)
    start_stay = jnp.zeros((head_count, query_count), jnp.float32)
    running, stay_sum = lax.fori_loop(0, block_count, visit_block, (start_total, start_stay))
    return running.reshape(query_count, head_count * value_size).astype(jnp.bfloat16)


def split_heads(array, head_size):
    return array.reshape(array.shape[0], array.shape[1] // head_size, head_size)


def local(
    stream,
    query_small,
    key_small,
    value_small,
    query_large,
    key_large,
    value_large,
    key_bias,
    out_small,
    out_large,
    gain_one,
    shift_one,
    gain_two,
    shift_two,
    expert_pick,
    route_weight,
    w_gate,
    w_up,
    w_down,
):
    row_count = stream.shape[0]
    position = lax.axis_index("sp")
    gathered = (
        lax.all_gather(key_small, "sp", axis=0, tiled=True),
        lax.all_gather(value_small, "sp", axis=0, tiled=True),
        lax.all_gather(key_large, "sp", axis=0, tiled=True),
        lax.all_gather(value_large, "sp", axis=0, tiled=True),
        lax.all_gather(key_bias, "sp", axis=0, tiled=True),
    )
    att_small = stick_group(
        split_heads(query_small, HEAD_SMALL),
        split_heads(gathered[0], HEAD_SMALL),
        split_heads(gathered[1], HEAD_SMALL),
        gathered[4][:, 0],
        position,
    )
    att_large = stick_group(
        split_heads(query_large, HEAD_LARGE),
        split_heads(gathered[2], HEAD_LARGE),
        split_heads(gathered[3], HEAD_LARGE),
        gathered[4][:, 1],
        position,
    )
    partial_value = jnp.dot(att_small, out_small, preferred_element_type=jnp.float32)
    partial_value = partial_value + jnp.dot(
        att_large, out_large, preferred_element_type=jnp.float32
    )
    mixer_out = lax.psum(partial_value.astype(jnp.bfloat16), "tp").astype(jnp.float32)
    normed = layer_norm(
        ALPHA_RES * stream.astype(jnp.float32) + mixer_out, gain_one, shift_one
    ).astype(jnp.bfloat16)
    experts = w_gate.shape[0] * lax.axis_size("sp")
    capacity = 4 * row_count // experts
    tp_count = lax.axis_size("tp")
    tp_index = lax.axis_index("tp")
    per_lane = capacity // tp_count
    flat_picks = expert_pick.reshape(-1)
    one_hot = (flat_picks[:, None] == jnp.arange(experts, dtype=jnp.int32)[None, :]).astype(
        jnp.int32
    )
    slot_rank = jnp.sum((jnp.cumsum(one_hot, axis=0) - one_hot) * one_hot, axis=1)
    slot_index = (flat_picks * capacity + slot_rank).reshape(row_count, 2)

    def selector(first_slot, slot_count):
        target = (
            jnp.arange(experts, dtype=jnp.int32)[:, None] * capacity
            + first_slot
            + jnp.arange(slot_count, dtype=jnp.int32)[None, :]
        ).reshape(-1)
        return [target[:, None] == slot_index[None, :, pick_index] for pick_index in range(2)]

    own_select = selector(tp_index * per_lane, per_lane)
    all_select = selector(0, capacity)
    placing = (all_select[0] | all_select[1]).astype(jnp.bfloat16)
    outgoing = jnp.dot(placing, normed, preferred_element_type=jnp.float32).astype(jnp.bfloat16)
    arrived = lax.all_to_all(
        outgoing.reshape(experts, capacity, normed.shape[1]),
        "sp",
        split_axis=0,
        concat_axis=0,
        tiled=True,
    )
    flat_rows = arrived.reshape(-1, arrived.shape[2])
    gate = jnp.dot(flat_rows, w_gate[0], preferred_element_type=jnp.float32)
    upper = jnp.dot(flat_rows, w_up[0], preferred_element_type=jnp.float32)
    hidden = (jax.nn.silu(gate) * upper).astype(jnp.bfloat16)
    expert_terms = jnp.dot(hidden, w_down[0], preferred_element_type=jnp.float32).reshape(
        arrived.shape
    )
    summed = lax.psum_scatter(
        expert_terms.astype(jnp.bfloat16), "tp", scatter_dimension=1, tiled=True
    )
    returned = lax.all_to_all(summed, "sp", split_axis=0, concat_axis=0, tiled=True).reshape(
        experts * per_lane, normed.shape[1]
    )
    picked_first = jnp.einsum(
        "sr,sd->rd",
        own_select[0].astype(jnp.bfloat16),
        returned,
        preferred_element_type=jnp.float32,
    )
    picked_second = jnp.einsum(
        "sr,sd->rd",
        own_select[1].astype(jnp.bfloat16),
        returned,
        preferred_element_type=jnp.float32,
    )
    partial_mix = route_weight[:, 0:1] * picked_first + route_weight[:, 1:2] * picked_second
    expert_mix = lax.psum_scatter(
        partial_mix.astype(jnp.bfloat16), "tp", scatter_dimension=0, tiled=True
    ).astype(jnp.float32)
    own_count = row_count // tp_count
    own_rows = lax.dynamic_slice_in_dim(normed, tp_index * own_count, own_count, 0).astype(
        jnp.float32
    )
    return layer_norm(ALPHA_RES * own_rows + expert_mix, gain_two, shift_two).astype(jnp.bfloat16)


GROUPS = 4


def fast_kernel(
    dims,
    qs_ref, ks_ref, vs_ref, ql_ref, kl_ref, vl_ref, bias_ref, stream_ref, os_ref, ol_ref,
    g1_ref, b1_ref, g2_ref, b2_ref, pick_ref, route_ref, wg_ref, wu_ref, wd_ref,
    out_ref,
    qs, ks, vs, ql, kl, vl, bias, g1, b1, g2, b2, pick, route,
    pack_a, pack_v, bias8, aq, ak, av, rb, tot, lat, ao, ra, wos, wol, strm, pb, rp, st, rst, normed,
    place, chosen, xs, wsend, wrecv, ag, xn, wg, wu, wd, acc, hid,
    y3, y2, y1, y0, dr, ts, rr, zs, zr, fs, fr,
    load_sem, q_send, q_recv, a_send, a_recv, p_send, p_recv, s_send, s_recv,
    x_send, x_recv, w_send, w_recv, g_send, g_recv, e_send, e_recv, d_send, d_recv,
    t_send, t_recv, z_send, z_recv, f_send, f_recv,
):
    n_sp, n_tp, rows, cols, cap, hs, hl = dims
    f32, bf16 = jnp.float32, jnp.bfloat16
    sp = lax.axis_index("sp")
    tp = lax.axis_index("tp")
    core = lax.rem(sp, 2)
    chip = lax.div(sp, 2)
    sibling = sp + 1 - 2 * core
    n_z = n_sp // 2
    is_small = core == 0
    ffw = wg_ref.shape[2]
    width = n_tp * cols

    def mesh_copy(src, dst, send, recv, target):
        return pltpu.make_async_remote_copy(
            src_ref=src, dst_ref=dst, send_sem=send, recv_sem=recv,
            device_id=target, device_id_type=pl.DeviceIdType.MESH,
        )

    def landed(ref, sem):
        pltpu.make_async_copy(ref, ref, sem).wait()

    def sp_at(j):
        return (j, tp)

    def tp_at(j):
        return (sp, j)

    def flip(index, mask, count):
        total, bit = 0, 1
        while bit < count:
            digit = lax.rem(lax.div(index, bit), 2)
            total = total + bit * (1 - digit if mask & bit else digit)
            bit *= 2
        return total

    z_order = [flip(chip, m, n_z) for m in range(n_z)]
    peers = [flip(tp, m, n_tp) for m in range(n_tp)]
    out_peers = [*peers[:0:-1], peers[0]]

    barrier = pltpu.get_barrier_semaphore()
    for k in range(1, n_sp):
        pl.semaphore_signal(barrier, inc=1, device_id=sp_at(lax.rem(sp + k, n_sp)), device_id_type=pl.DeviceIdType.MESH)
    for k in range(1, n_tp):
        pl.semaphore_signal(barrier, inc=1, device_id=tp_at(lax.rem(tp + k, n_tp)), device_id_type=pl.DeviceIdType.MESH)

    own_cols = pl.ds(pl.multiple_of(tp * cols, cols), cols)
    own_ff = pl.ds(pl.multiple_of(core * ffw, ffw), ffw)
    pairs = [
        (qs_ref, qs), (ks_ref, ks), (vs_ref, vs), (ql_ref, ql), (kl_ref, kl), (vl_ref, vl), (bias_ref, bias),
        (g1_ref, g1), (b1_ref, b1), (g2_ref, g2), (b2_ref, b2), (pick_ref, pick), (route_ref, route),
        (stream_ref.at[:, own_cols], strm), (os_ref, wos), (ol_ref, wol),
        (wg_ref.at[0], wg.at[core]), (wu_ref.at[0], wu.at[core]), (wd_ref.at[0], wd.at[own_ff]),
    ]
    loads = [pltpu.make_async_copy(src, dst, load_sem.at[n]) for n, (src, dst) in enumerate(pairs)]
    for load in loads[:13]:
        load.start()
    for load in loads[:7]:
        load.wait()

    for h in range(n_z):
        part = slice(h * hs, (h + 1) * hs)
        pack_a[h] = jnp.concatenate([qs[:, part], ks[:, part]], axis=1)
        pack_v[h] = jnp.concatenate([vs[:rows // 2, part], vs[rows // 2:, part]], axis=1)
        for kind in range(2):
            bias8[kind * n_z + h] = jnp.broadcast_to(bias[kind, h:h + 1, :].astype(f32), (8, rows))

    pl.semaphore_wait(barrier, n_sp + n_tp - 2)

    half_block = pl.ds(0, rows // 2)
    top = pl.ds(0, 1)

    def head_parts(kind, h, slot):
        if kind == 0:
            return [
                (0, pack_a.at[h], aq.at[slot]),
                (2, pack_v.at[h], av.at[slot, half_block]),
                (3, bias8.at[h, top], rb.at[slot, top]),
            ]
        part = pl.ds(pl.multiple_of(h * hl, hl), hl)
        return [
            (0, ql.at[:, part], aq.at[slot]),
            (1, kl.at[:, part], ak.at[slot]),
            (2, vl.at[:, part], av.at[slot]),
            (3, bias8.at[n_z + h, top], rb.at[slot, top]),
        ]

    def head_copies(z, kind):
        d = 2 * z + kind
        return [
            mesh_copy(src, dst, q_send.at[n, d], q_recv.at[n, sp], sp_at(d))
            for n, src, dst in head_parts(kind, z, sp)
        ]

    def for_targets(act):
        for kind in range(2):
            @pl.when(core != kind)
            def _():
                act(head_copies(chip, kind))
        for distance in range(1, n_z):
            for sign in (1, -1):
                z = chip + sign * distance

                @pl.when((z >= 0) & (z < n_z))
                def _():
                    for kind in range(2):
                        act(head_copies(z, kind))

    def start_all(copies):
        for copy in copies:
            copy.start()

    def sent_all(copies):
        for copy in copies:
            copy.wait_send()

    for_targets(start_all)
    for kind in range(2):
        @pl.when(core == kind)
        def _():
            for n, src, dst in head_parts(kind, chip, sp):
                pltpu.make_async_copy(src, dst, q_recv.at[n, sp]).start()

    for load in loads[13:]:
        load.start()
    weights = [
        mesh_copy(wg_ref.at[0], wg.at[core], e_send.at[0], e_recv.at[0], sp_at(sibling)),
        mesh_copy(wu_ref.at[0], wu.at[core], e_send.at[1], e_recv.at[1], sp_at(sibling)),
        mesh_copy(wd_ref.at[0], wd.at[own_ff], e_send.at[2], e_recv.at[2], sp_at(sibling)),
    ]
    start_all(weights)

    for load in loads[7:13]:
        load.wait()
    group = lax.div(pick[0:1, :], 2)
    first_even = lax.rem(pick[0:1, :], 2) == 0
    sub8 = lax.broadcasted_iota(jnp.int32, (8, rows), 0)
    one_hot = (sub8 == group).astype(f32)
    sub_r = lax.broadcasted_iota(jnp.int32, (rows, rows), 0)
    lane_r = lax.broadcasted_iota(jnp.int32, (rows, rows), 1)
    before = (sub_r < lane_r).astype(f32).astype(bf16)
    counts = jnp.dot(one_hot.astype(bf16), before, preferred_element_type=f32)
    rank = jnp.sum(one_hot * counts, axis=0, keepdims=True).astype(jnp.int32)
    slot_row = group * cap + rank
    slot_iota = lax.broadcasted_iota(jnp.int32, (GROUPS * cap, rows), 0)
    place[...] = (slot_iota == slot_row).astype(f32).astype(bf16)
    for g in range(GROUPS):
        chosen[g] = ((sub_r == slot_row - g * cap) & (sub_r < cap)).astype(f32).astype(bf16)

    def unfold(packed):
        tall = jnp.concatenate([packed[:, :hs], packed[:, hs:]], axis=0)
        return jnp.concatenate([tall, jnp.zeros_like(tall)], axis=1)

    lane_h = lax.broadcasted_iota(jnp.int32, (rows, hl), 1)

    def take(z):
        for half in range(2):
            j = 2 * z + half
            landed(rb.at[j, top], q_recv.at[3, j])
            landed(aq.at[j], q_recv.at[0, j])

            @pl.when(is_small)
            def _():
                folded = av.at[j, half_block]
                landed(folded, q_recv.at[2, j])
                both = aq[j]
                ak[j] = jnp.concatenate([both[:, hs:], both[:, :hs]], axis=1)
                aq[j] = jnp.where(lane_h < hs, both, jnp.zeros_like(both))
                av[j] = unfold(folded[...])

            @pl.when(jnp.logical_not(is_small))
            def _():
                landed(ak.at[j], q_recv.at[1, j])
                landed(av.at[j], q_recv.at[2, j])

    scale = jnp.where(is_small, hs**-0.5, hl**-0.5).astype(f32)
    span = 2 * rows
    sub_t = lax.broadcasted_iota(jnp.int32, (span, span), 0)
    lane_t = lax.broadcasted_iota(jnp.int32, (span, span), 1)
    tri = (sub_t >= lane_t).astype(f32).astype(bf16)
    causal = lane_t < sub_t

    def pair_of(ref, z):
        return ref[pl.ds(2 * z, 2)].reshape(span, hl)

    def tile(q, k, diagonal, later):
        log_odds = jnp.concatenate([rb[2 * k, 0:1, :], rb[2 * k + 1, 0:1, :]], axis=1)
        score = lax.dot_general(
            pair_of(aq, q), pair_of(ak, k), (((1,), (1,)), ((), ())), preferred_element_type=f32
        )
        score = score * scale + log_odds
        soft = jnp.maximum(score, 0.0) + jnp.log(1.0 + jnp.exp(-jnp.abs(score)))
        if diagonal:
            soft = jnp.where(causal, soft, 0.0)
        high = soft.astype(bf16)
        low = (soft - high.astype(f32)).astype(bf16)
        run = jnp.dot(high, tri, preferred_element_type=f32) + jnp.dot(low, tri, preferred_element_type=f32)
        if diagonal:
            stick = jnp.where(causal, jnp.exp(score - run), 0.0)
        else:
            stick = jnp.exp(score - run - later)
        added = jnp.dot(stick.astype(bf16), pair_of(av, k), preferred_element_type=f32)
        return added, run[:, 0:1]

    def head_back(d, small):
        src, dst = (ao.at[d, half_block], ra.at[sp, half_block]) if small else (ao.at[d], ra.at[sp])
        return src, dst, mesh_copy(src, dst, a_send.at[d], a_recv.at[sp], sp_at(d))

    def finish(q):
        for half in range(2):
            d = 2 * q + half
            block = tot[q, half * rows:(half + 1) * rows].astype(bf16)
            for small in (True, False):
                @pl.when(is_small if small else jnp.logical_not(is_small))
                def _():
                    if small:
                        ao[d, :rows // 2, :] = jnp.concatenate([block[:rows // 2, :hs], block[rows // 2:, :hs]], axis=1)
                    else:
                        ao[d] = block
                    src, dst, copy = head_back(d, small)

                    @pl.when(d != sp)
                    def _():
                        copy.start()

                    @pl.when(d == sp)
                    def _():
                        pltpu.make_async_copy(src, dst, a_recv.at[d]).start()

    lower = chip < n_z // 2
    mirrored = jnp.where(lower, chip, n_z - 1 - chip)
    for s in range(n_z):
        if s == 0:
            turn = mirrored
        elif s == 1:
            turn = 1 - mirrored
        else:
            turn = s
        z = jnp.where(lower, turn, n_z - 1 - turn)
        rising = lower if s != 1 else (lower == (mirrored == 0))
        take(z)
        added, current = tile(z, z, True, None)
        tot[z] = added
        lat[z] = current
        for i in range(1, s + 1):
            q = jnp.where(rising, z, z + i)
            k = jnp.where(rising, z - i, z)
            later = lat[q]
            added, current = tile(q, k, False, later)
            tot[q] = tot[q] + added
            lat[q] = later + current
        if s == 0:
            @pl.when(lower & (mirrored == 0))
            def _():
                finish(0)
        elif s == 1:
            @pl.when(lower & (mirrored == 1))
            def _():
                finish(0)

            @pl.when(lower)
            def _():
                finish(1)
        elif s < n_z - 1:
            @pl.when(lower)
            def _():
                finish(s)
        else:
            @pl.when(lower)
            def _():
                finish(s)

            @pl.when(jnp.logical_not(lower))
            def _():
                for q in range(n_z):
                    finish(q)

    for load in loads[13:16]:
        load.wait()
    for j in range(n_sp):
        landed(ra.at[j] if j % 2 else ra.at[j, half_block], a_recv.at[j])
    att_small = jnp.concatenate([unfold(ra[2 * h, :rows // 2, :])[:, :hs] for h in range(n_z)], axis=1)
    att_large = jnp.concatenate([ra[2 * h + 1] for h in range(n_z)], axis=1)

    for k in range(1, n_tp + 1):
        t = out_peers[k - 1]
        part = pl.ds(pl.multiple_of(t * cols, cols), cols)
        term = jnp.dot(att_small, wos[:, part], preferred_element_type=f32)
        term = term + jnp.dot(att_large, wol[:, part], preferred_element_type=f32)
        pb[k - 1] = term.astype(bf16)
        if k < n_tp:
            mesh_copy(pb.at[k - 1], rp.at[tp], p_send.at[k], p_recv.at[tp], tp_at(t)).start()
    mixed = ALPHA_RES * strm[...].astype(f32) + pb[n_tp - 1].astype(f32)
    for k in range(1, n_tp):
        landed(rp.at[peers[k]], p_recv.at[peers[k]])
        mixed = mixed + rp[peers[k]].astype(f32)

    eye = sub_r == lane_r

    def to_row(column):
        return jnp.sum(jnp.where(eye, column, 0.0), axis=0, keepdims=True)

    def to_column(row):
        return jnp.sum(jnp.where(eye, row, 0.0), axis=1, keepdims=True)

    own_mean = jnp.mean(mixed, axis=1, keepdims=True)
    centred = mixed - own_mean
    own_square = jnp.sum(centred * centred, axis=1, keepdims=True)
    mean_row, square_row = to_row(own_mean), to_row(own_square)
    st[...] = jnp.where(sub8 == 0, mean_row, square_row)
    for k in range(1, n_tp):
        mesh_copy(st, rst.at[tp], s_send.at[k], s_recv.at[tp], tp_at(peers[k])).start()

    sent = centred.astype(bf16)
    for g in range(GROUPS):
        xs[g] = jnp.dot(place[g * cap:(g + 1) * cap, :], sent, preferred_element_type=f32).astype(bf16)

    def x_copy(k):
        z = z_order[k]
        return mesh_copy(xs.at[z], ag.at[tp, chip], x_send.at[k], x_recv.at[chip], sp_at(2 * z + core))

    def g_copy(m, k):
        z = z_order[k]
        src = xs.at[chip] if k == 0 else ag.at[tp, z]
        return mesh_copy(src, ag.at[tp, z], g_send.at[m, z], g_recv.at[tp, z], tp_at(peers[m]))

    def g_relay(k):
        z = z_order[k]
        m = 1 if k < n_z // 2 else 2
        piece = ag.at[peers[m], z]
        return mesh_copy(piece, piece, g_send.at[3, z], g_recv.at[peers[m], z], tp_at(peers[3 - m]))

    def relay(k):
        m = 1 if k < n_z // 2 else 2
        landed(ag.at[peers[m], z_order[k]], g_recv.at[peers[m], z_order[k]])
        g_relay(k).start()

    for k in range(1, n_z):
        x_copy(k).start()
    pltpu.make_async_copy(xs.at[chip], ag.at[tp, chip], x_recv.at[chip]).start()
    for m in (1, 2):
        g_copy(m, 0).start()

    means, squares = [(tp, mean_row)], [square_row]
    for k in range(1, n_tp):
        src = peers[k]
        landed(rst.at[src], s_recv.at[src])
        means.append((src, rst[src, 0:1, :]))
        squares.append(rst[src, 1:2, :])
    full_mean = sum(m for _, m in means) / n_tp
    spread = sum(squares) + cols * sum((m - full_mean) * (m - full_mean) for _, m in means)
    scale_row = lax.rsqrt(spread / width + NORM_EPS)

    w_even = jnp.where(first_even, route[0:1, :], route[1:2, :])
    w_odd = jnp.where(first_even, route[1:2, :], route[0:1, :])
    w8 = jnp.where(sub8 == 0, w_even, jnp.where(sub8 == 1, w_odd, jnp.where(sub8 == 2, scale_row, 0.0)))
    for src, m in means:
        w8 = jnp.where(sub8 == 3 + src, m - full_mean, w8)
    w_hi = w8.astype(bf16)
    w_lo = (w8 - w_hi.astype(f32)).astype(bf16)
    last = (((1,), (1,)), ((), ()))
    for g in range(GROUPS):
        wsend[g] = lax.dot_general(w_hi, chosen[g], last, preferred_element_type=f32) + lax.dot_general(
            w_lo, chosen[g], last, preferred_element_type=f32
        )

    def w_copy(k):
        z = z_order[k]
        return mesh_copy(wsend.at[z], wrecv.at[chip], w_send.at[k], w_recv.at[chip], sp_at(2 * z + core))

    for k in range(1, n_z):
        w_copy(k).start()
    pltpu.make_async_copy(wsend.at[chip], wrecv.at[chip], w_recv.at[chip]).start()

    norm_val = (mixed - to_column(full_mean)) * to_column(scale_row) * g1[:, own_cols] + b1[:, own_cols]
    normed[...] = norm_val.astype(bf16)

    for k in range(n_z):
        landed(ag.at[tp, z_order[k]], x_recv.at[z_order[k]])
        if k:
            for m in (1, 2):
                g_copy(m, k).start()
        if k and k <= n_z // 2:
            relay(k - 1)
    for z in range(n_z):
        landed(wrecv.at[z], w_recv.at[z])
    for load in loads[16:]:
        load.wait()
    for copy in weights:
        copy.wait_recv()
    lane_c = lax.broadcasted_iota(jnp.int32, (cap, rows), 1)
    sub_c = lax.broadcasted_iota(jnp.int32, (cap, rows), 0)

    def slot_column(z, r):
        return jnp.sum(jnp.where(sub_c == lane_c, wrecv[z, pl.ds(r, 1), :], 0.0), axis=1, keepdims=True)

    rate = [slot_column(z, 2) for z in range(n_z)]
    slot_weight = [jnp.concatenate([slot_column(z, e) for z in range(n_z)], axis=0) for e in range(2)]
    step = min(512, ffw)

    def spread_in(m):
        t = peers[m]
        part = pl.ds(pl.multiple_of(t * cols, cols), cols)
        gain, shift = g1[:, part], b1[:, part]
        for z in range(n_z):
            value = (ag[t, z].astype(f32) + slot_column(z, 3 + t)) * rate[z] * gain + shift
            xn[z * cap:(z + 1) * cap, :] = value.astype(bf16)

    def up_half(m, e):
        inner = pl.ds(pl.multiple_of(peers[m] * cols, cols), cols)
        x = xn[...]
        for n in range(ffw // step):
            part = slice(n * step, (n + 1) * step)
            gate = jnp.dot(x, wg[e, inner, part], preferred_element_type=f32)
            upper = jnp.dot(x, wu[e, inner, part], preferred_element_type=f32)
            if m:
                gate = gate + acc[e, 0, :, part]
                upper = upper + acc[e, 1, :, part]
            if m < n_tp - 1:
                acc[e, 0, :, part] = gate
                acc[e, 1, :, part] = upper
            else:
                value = gate / (1.0 + jnp.exp(-gate)) * upper * slot_weight[e]
                hid[:, e * ffw + n * step:e * ffw + (n + 1) * step] = value.astype(bf16)

    def arrive(m, ks):
        for k in ks:
            landed(ag.at[peers[m], z_order[k]], g_recv.at[peers[m], z_order[k]])

    spread_in(0)
    up_half(0, 0)
    relay(2)
    up_half(0, 1)
    relay(3)
    arrive(1, (2, 3))
    spread_in(1)
    up_half(1, 0)
    up_half(1, 1)
    arrive(2, (0, 1))
    spread_in(2)
    up_half(2, 0)
    up_half(2, 1)
    arrive(3, range(n_z))
    spread_in(3)
    up_half(3, 0)
    up_half(3, 1)

    far, near = z_order[:1:-1], z_order[1::-1]

    def down(m):
        part = pl.ds(pl.multiple_of(peers[m] * cols, cols), cols)
        return jnp.dot(hid[...], wd[:, part], preferred_element_type=f32)

    def d_copy(m, z):
        return mesh_copy(y3.at[z], dr.at[m - 1, z], d_send.at[m - 1, z], d_recv.at[m - 1, z], tp_at(peers[m]))

    def t_copy(m, z):
        return mesh_copy(ts.at[m - 1, z], rr.at[m - 1, z], t_send.at[m - 1, z], t_recv.at[m - 1, z], tp_at(peers[m]))

    y3[...] = down(3).astype(bf16).reshape(n_z, cap, cols)
    for a, b in zip(far, near):
        d_copy(1, a).start()
        d_copy(2, b).start()
    y2[...] = down(2).reshape(n_z, cap, cols)
    for z in near:
        ts[1, z] = y2[z].astype(bf16)
        t_copy(2, z).start()
    y1[...] = down(1).reshape(n_z, cap, cols)
    for z in far:
        ts[0, z] = y1[z].astype(bf16)
        t_copy(1, z).start()
    y0[...] = down(0).reshape(n_z, cap, cols)
    for a, b in zip(far, near):
        landed(dr.at[0, a], d_recv.at[0, a])
        ts[1, a] = (y2[a] + dr[0, a].astype(f32)).astype(bf16)
        t_copy(2, a).start()
        landed(dr.at[1, b], d_recv.at[1, b])
        ts[0, b] = (y1[b] + dr[1, b].astype(f32)).astype(bf16)
        t_copy(1, b).start()

    def z_copy(z):
        return mesh_copy(zs.at[z], zr.at[chip], z_send.at[z], z_recv.at[chip], sp_at(2 * z + core))

    for k, z in enumerate([*far, *near]):
        for m in range(2):
            landed(rr.at[m, z], t_recv.at[m, z])
        zs[z] = (y0[z] + rr[0, z].astype(f32) + rr[1, z].astype(f32)).astype(bf16)
        if k < n_z - 1:
            z_copy(z).start()
        else:
            pltpu.make_async_copy(zs.at[z], zr.at[chip], z_recv.at[chip]).start()
    for z in range(n_z):
        landed(zr.at[z], z_recv.at[z])
    expert_mix = lax.dot_general(
        place[...], zr[...].reshape(n_z * cap, cols), (((0,), (0,)), ((), ())), preferred_element_type=f32
    )
    final = ALPHA_RES * normed[...].astype(f32) + expert_mix
    own_rows = rows // n_tp
    middle = jnp.mean(final, axis=1, keepdims=True)
    middle_hi = middle.astype(bf16)
    middle_lo = (middle - middle_hi.astype(f32)).astype(bf16)
    packed = (final - (middle_hi.astype(f32) + middle_lo.astype(f32))).astype(bf16)
    extra = jnp.where(lane_h < hs, middle_hi.astype(f32), middle_lo.astype(f32)).astype(bf16)
    for t in range(n_tp):
        fs[t, :, :cols] = packed[t * own_rows:(t + 1) * own_rows]
        fs[t, :, cols:] = extra[t * own_rows:(t + 1) * own_rows]

    def f_copy(k):
        return mesh_copy(fs.at[peers[k]], fr.at[tp], f_send.at[k], f_recv.at[tp], tp_at(peers[k]))

    for k in range(n_tp - 1, 0, -1):
        f_copy(k).start()
    pltpu.make_async_copy(fs.at[tp], fr.at[tp], f_recv.at[tp]).start()
    for t in range(n_tp):
        landed(fr.at[t], f_recv.at[t])
    blocks = []
    for t in range(n_tp):
        tail = fr[t, :, cols:].astype(f32)
        blocks.append(fr[t, :, :cols].astype(f32) + (tail[:, 0:1] + tail[:, hs:hs + 1]))
    average = sum(jnp.sum(b, axis=1, keepdims=True) for b in blocks) / width
    blocks = [b - average for b in blocks]
    variance = sum(jnp.sum(b * b, axis=1, keepdims=True) for b in blocks) / width
    inverse = lax.rsqrt(variance + NORM_EPS)
    for t in range(n_tp):
        part = slice(t * cols, (t + 1) * cols)
        out_ref[:, part] = (blocks[t] * inverse * g2[:, part] + b2[:, part]).astype(bf16)

    for_targets(sent_all)
    sent_all(weights)
    for d in range(n_sp):
        for small in (True, False):
            @pl.when((d != sp) & (is_small if small else jnp.logical_not(is_small)))
            def _():
                head_back(d, small)[2].wait_send()
    for k in range(1, n_tp):
        mesh_copy(pb.at[k - 1], rp.at[tp], p_send.at[k], p_recv.at[tp], tp_at(out_peers[k - 1])).wait_send()
        mesh_copy(st, rst.at[tp], s_send.at[k], s_recv.at[tp], tp_at(peers[k])).wait_send()
        f_copy(k).wait_send()
    for k in range(1, n_z):
        x_copy(k).wait_send()
        w_copy(k).wait_send()
    for k in range(n_z):
        g_copy(1, k).wait_send()
        g_copy(2, k).wait_send()
        g_relay(k).wait_send()
    for a, b in zip(far, near):
        d_copy(1, a).wait_send()
        d_copy(2, b).wait_send()
    for z in z_order:
        t_copy(1, z).wait_send()
        t_copy(2, z).wait_send()
    for z in z_order[1:]:
        z_copy(z).wait_send()


def fast_local(
    stream, query_small, key_small, value_small, query_large, key_large, value_large, key_bias,
    out_small, out_large, gain_one, shift_one, gain_two, shift_two, expert_pick, route_weight,
    w_gate, w_up, w_down,
):
    f32, bf16 = jnp.float32, jnp.bfloat16
    n_sp, n_tp = lax.axis_size("sp"), lax.axis_size("tp")
    rows, width = stream.shape
    cols = width // n_tp
    hs, hl = HEAD_SMALL, HEAD_LARGE
    cap = 4 * rows // (w_gate.shape[0] * n_sp)
    n_z = n_sp // 2
    ffw = w_gate.shape[2]
    hbm = pl.BlockSpec(memory_space=pl.ANY)
    dma = pltpu.SemaphoreType.DMA
    V = pltpu.VMEM
    slots = n_z * cap
    operands = (
        query_small, key_small, value_small, query_large, key_large, value_large,
        key_bias.transpose(1, 2, 0), stream, out_small, out_large,
        gain_one[None], shift_one[None], gain_two[None], shift_two[None],
        expert_pick.T, route_weight.T, w_gate, w_up, w_down,
    )
    kept = [*operands[:7], *operands[10:16]]
    scratch = [
        *[V(a.shape, a.dtype) for a in kept],
        V((n_z, rows, hl), bf16), V((n_z, rows // 2, hl), bf16), V((n_sp, 8, rows), f32),
        V((n_sp, rows, hl), bf16), V((n_sp, rows, hl), bf16), V((n_sp, rows, hl), bf16),
        V((n_sp, 8, rows), f32),
        V((n_z, 2 * rows, hl), f32), V((n_z, 2 * rows, 1), f32),
        V((n_sp, rows, hl), bf16), V((n_sp, rows, hl), bf16),
        V(out_small.shape, bf16), V(out_large.shape, bf16), V((rows, cols), bf16),
        V((n_tp, rows, cols), bf16), V((n_tp, rows, cols), bf16),
        V((8, rows), f32), V((n_tp, 8, rows), f32), V((rows, cols), bf16),
        V((GROUPS * cap, rows), bf16), V((GROUPS, rows, rows), bf16), V((GROUPS, cap, cols), bf16),
        V((GROUPS, 8, rows), f32), V((n_z, 8, rows), f32),
        V((n_tp, n_z, cap, cols), bf16), V((slots, cols), bf16),
        V((2, width, ffw), bf16), V((2, width, ffw), bf16), V((2 * ffw, width), bf16),
        V((2, 2, slots, ffw), f32), V((slots, 2 * ffw), bf16),
        V((n_z, cap, cols), bf16), V((n_z, cap, cols), f32), V((n_z, cap, cols), f32), V((n_z, cap, cols), f32),
        V((2, n_z, cap, cols), bf16), V((2, n_z, cap, cols), bf16), V((2, n_z, cap, cols), bf16),
        V((n_z, cap, cols), bf16), V((n_z, cap, cols), bf16),
        V((n_tp, rows // n_tp, cols + hl), bf16), V((n_tp, rows // n_tp, cols + hl), bf16),
        dma((19,)), dma((4, n_sp)), dma((4, n_sp)), dma((n_sp,)), dma((n_sp,)),
        dma((n_tp,)), dma((n_tp,)), dma((n_tp,)), dma((n_tp,)),
        dma((n_z,)), dma((n_z,)), dma((n_z,)), dma((n_z,)),
        dma((n_tp, n_z)), dma((n_tp, n_z)), dma((3,)), dma((3,)),
        dma((2, n_z)), dma((2, n_z)), dma((2, n_z)), dma((2, n_z)),
        dma((n_z,)), dma((n_z,)), dma((n_tp,)), dma((n_tp,)),
    ]
    dims = (n_sp, n_tp, rows, cols, cap, hs, hl)
    return pl.pallas_call(
        functools.partial(fast_kernel, dims),
        out_shape=jax.ShapeDtypeStruct((rows // n_tp, width), bf16),
        in_specs=[hbm] * len(operands),
        out_specs=pl.BlockSpec(memory_space=pltpu.VMEM),
        scratch_shapes=scratch,
        compiler_params=pltpu.CompilerParams(
            collective_id=0, has_side_effects=True, vmem_limit_bytes=60 * 1024 * 1024
        ),
        name="layer",
    )(*operands)


def layer(*arrays):
    n_sp, n_tp = lax.axis_size("sp"), lax.axis_size("tp")
    rows, width = arrays[0].shape
    small, large = arrays[1].shape[1] // HEAD_SMALL, arrays[4].shape[1] // HEAD_LARGE
    experts = arrays[16].shape[0] * n_sp
    paired = experts == 2 * GROUPS and n_sp == experts and n_tp == GROUPS
    if paired and small == large and 2 * small == n_sp and rows == HEAD_LARGE and width % (128 * n_tp) == 0:
        return fast_local(*arrays)
    return local(*arrays)


def solution(mesh):
    placed = (
        P("sp", None),
        P("sp", "tp"),
        P("sp", "tp"),
        P("sp", "tp"),
        P("sp", "tp"),
        P("sp", "tp"),
        P("sp", "tp"),
        P("sp", None, "tp"),
        P("tp", None),
        P("tp", None),
        P(),
        P(),
        P(),
        P(),
        P("sp", None),
        P("sp", None),
        P("sp", None, "tp"),
        P("sp", None, "tp"),
        P("sp", "tp", None),
    )
    return jax.shard_map(
        layer, mesh=mesh, in_specs=placed, out_specs=P(("sp", "tp"), None), check_vma=False
    )
```

time: 92.9 us -> 76.8 us (0.83)
  Pallas kernels: 89.8 us -> 75.1 us
    pallas_call x1, Pallas kernels: 89.8 us -> 75.1 us  [fast_local(): pl.pallas_call(functools.partial(fast_kernel, dims), out_shape=jax.ShapeD...]
where the time goes in v1:
time: 76.8 us; the launch traced here: 76.6 us
  Pallas kernels  75.1 us (98%)
  local copies, waits for them, and re-layouts  1.57 us (2%)
    pallas_call x1, Pallas kernels, fast_local(): pl.pallas_call(functools.partial(fast_kernel, dims), out_shape=jax.ShapeD...  75.1 us
    unnamed x1, local copies, waits for them, and re-layouts  1.57 us

profile of v1, /device:TPU:0, one launch (start us, length us, event | category | flops | bytes accessed | tf_op | source)
XLA Modules:
  0.0 76.6 jit_solution(16885269280958137947)
XLA Ops:
  0.0 75.1 %layer.1 = bf16[32,2048]{1,0:T(8,128)(2,1)} custom-call(bf16[128,256]{1,0:T(8,128)(2,1)} %qs_ref.1, bf16[128,256]{1,0:T(8,128)(2,1)} %ks_ref.1, bf16[128,256]{1,0:T(8,128)(2,1)} %vs_ref.1, bf16[128,512]{1,0:T(8,128)(2,1)} %ql_ref.1, bf16[128,512]{1,0:T(8,128)(2,1)} %kl_ref.1, bf16[128,512]{1,0:T(8,128)(2,1)} %vl_ref.1, bf16[2,4,128]{2,1,0:T(4,128)(2,1)} %bitcast.11, ...), custom_call_target="tpu_custom_call" | custom-call | tf_op jit(solution)/shard_map/layer/pallas_call | solution.py:805
  75.1 1.6 %copy.21 = bf16[32,2048]{1,0:T(8,128)(2,1)} copy(bf16[32,2048]{1,0:T(8,128)(2,1)} %layer.1) | data formatting | bytes 262144
